TPU v7x, 256 devices: a whole 4x4x8 slice. The times are simulated.
256 devices in a mesh: ep: 64 (over z, y, core), tp: 4 (over x).
Axes of the slice: x: 4, y: 4, z: 8, core: 2. Of those that a mesh axis runs over, the one named last changes fastest.
Arguments:
- first_input: bfloat16 [32768, 2048], P('ep'), may hold values from -120 to 120
- first_gain: bfloat16 [2048], replicated, may hold values from 0.099609375 to 1.8984375
- pool_inward: bfloat16 [2048, 1024], P(None, 'tp'), may hold values from -0.125 to 0.125
- pool_mixing: bfloat16 [4, 256, 256], P('tp'), may hold values from -0.375 to 0.375
- pool_scale: bfloat16 [1024], P('tp'), may hold values from 0.099609375 to 1.8984375
- pool_outward: bfloat16 [1024, 2048], P('tp'), may hold values from -0.1875 to 0.1875
- second_input: bfloat16 [16384, 2048], P('ep'), may hold values from -120 to 120
- second_gain: bfloat16 [2048], replicated, may hold values from 0.099609375 to 1.8984375
- route_ids: int32 [16384, 2], P('ep'), may hold values from 0 to 31, all different within a row; in each aligned block of 256 rows (0 to 255, 256 to 511, ...) at most 18 rows name the same one
- route_logits: float32 [16384, 2], P('ep'), may hold values from -6 to 6
- expert_gate: bfloat16 [64, 2048, 2048], P('ep', None, 'tp'), may hold values from -0.125 to 0.125
- expert_up: bfloat16 [64, 2048, 2048], P('ep', None, 'tp'), may hold values from -0.125 to 0.125
- expert_down: bfloat16 [64, 2048, 2048], P('ep', 'tp'), may hold values from -0.09375 to 0.09375
Outputs:
- first_out: bfloat16 [32768, 2048], P('ep', 'tp')
- second_out: bfloat16 [16384, 2048], P('ep', 'tp')
Inputs may be any that keep to these rules, and one draw needn't show every extreme that they name: `route_ids`: each row names two different experts. In each aligned block of 256 rows (the rows of one index of ep) no expert is named by more than 18 rows, and in some blocks one expert is named by exactly 18 rows.
All inputs are finite; a program needn't handle non-finite values.
Results may differ from a plain program's by a relative error of at most 0.012.
Values may be sent and summed in bfloat16 or wider, within the bound.
No kernel may reach another device: no remote copies, remote signals or barrier semaphores. Data moves between devices by JAX's collectives and lax.ppermute only.
A program may use at most 64 MiB of HBM per device.

v0:
```python
import jax
import jax.numpy as jnp
from jax import lax
from jax.sharding import Mesh, PartitionSpec as P

epsilon = 1e-06


def from_behind(value, axis, steps):
    count = lax.axis_size(axis)
    leading, last = (max(0, -steps), min(count, count - steps))
    return lax.ppermute(value, axis, [(source, source + steps) for source in range(leading, last)])


def rms_scaled(values, weights):
    widened = values.astype(jnp.float32)
    inverse = lax.rsqrt(jnp.mean(widened * widened, axis=-1, keepdims=True) + epsilon)
    return (widened * inverse * weights.astype(jnp.float32)).astype(jnp.bfloat16)


def window_means(channels, length, offset):
    row_count = channels.shape[0] - 15
    summed = jnp.zeros((row_count, channels.shape[1]), jnp.float32)
    for lookback in range(16):
        summed = summed + jnp.where(
            lookback < length, channels[15 - lookback : 15 - lookback + row_count], 0.0
        )
    positions = offset + jnp.arange(row_count, dtype=jnp.int32)
    counts = jnp.minimum(positions + 1, length).astype(jnp.float32)
    return summed / counts[:, None]


def slot_positions(block_ids, expert_count, capacity):
    flattened = block_ids.reshape(-1)
    onehot = (flattened[:, None] == jnp.arange(expert_count, dtype=jnp.int32)[None, :]).astype(
        jnp.int32
    )
    running = jnp.cumsum(onehot, axis=0, dtype=jnp.int32) - 1
    slot_numbers = jnp.sum(onehot * running, axis=1)
    return flattened * capacity + slot_numbers


def expert_output(gate_sum, up_sum, down_rows):
    hidden = (jax.nn.silu(gate_sum) * up_sum).astype(jnp.bfloat16)
    return jnp.dot(hidden, down_rows, preferred_element_type=jnp.float32)


def local(
    first_input,
    first_gain,
    pool_inward,
    pool_mixing,
    pool_scale,
    pool_outward,
    second_input,
    second_gain,
    route_ids,
    route_logits,
    expert_gate,
    expert_up,
    expert_down,
):
    tensor_parts = lax.axis_size("tp")
    expert_count = lax.axis_size("z") * lax.axis_size("y")
    model_width = first_input.shape[1]
    quarter_width = model_width // tensor_parts
    swap = [(0, 1), (1, 0)]
    gate_other = lax.ppermute(expert_gate[0], "core", swap)
    up_other = lax.ppermute(expert_up[0], "core", swap)
    down_other = lax.ppermute(expert_down[0], "core", swap)
    normed_first = rms_scaled(first_input, first_gain)
    pooled_in = jnp.dot(normed_first, pool_inward, preferred_element_type=jnp.float32).astype(
        jnp.bfloat16
    )
    halo_rows = from_behind(pooled_in[-15:], ("z", "y", "core"), 1)
    extended = jnp.concatenate([halo_rows, pooled_in], axis=0).astype(jnp.float32)
    window = jnp.left_shift(jnp.int32(2), lax.axis_index("tp"))
    sequence_start = lax.axis_index(("z", "y", "core")) * first_input.shape[0]
    means = window_means(extended, window, sequence_start)
    mixed = (means - pooled_in.astype(jnp.float32)).astype(jnp.bfloat16)
    pooled = (
        jnp.dot(mixed, pool_mixing[0], preferred_element_type=jnp.float32)
        * pool_scale.astype(jnp.float32)
    ).astype(jnp.bfloat16)
    mixer_term = jnp.dot(pooled, pool_outward, preferred_element_type=jnp.float32)
    normed_second = rms_scaled(second_input, second_gain)
    row_count = second_input.shape[0]
    capacity = 2 * row_count * 9 // (8 * expert_count)
    positions = slot_positions(route_ids, expert_count, capacity)
    quarter = lax.dynamic_slice_in_dim(
        normed_second, lax.axis_index("tp") * quarter_width, quarter_width, 1
    )
    repeated = jnp.repeat(quarter, 2, axis=0)
    buffer = (
        jnp.zeros((expert_count * capacity, quarter_width), jnp.bfloat16)
        .at[positions]
        .set(repeated)
        .reshape(expert_count, capacity, quarter_width)
    )
    arrived = lax.all_to_all(buffer, ("z", "y"), split_axis=0, concat_axis=0, tiled=True)
    flattened = arrived.reshape(-1, quarter_width)
    portion = lax.all_gather(flattened, "tp", axis=1, tiled=True)
    flat_term = expert_output(
        jnp.dot(portion, expert_gate[0], preferred_element_type=jnp.float32),
        jnp.dot(portion, expert_up[0], preferred_element_type=jnp.float32),
        expert_down[0],
    ) + expert_output(
        jnp.dot(portion, gate_other, preferred_element_type=jnp.float32),
        jnp.dot(portion, up_other, preferred_element_type=jnp.float32),
        down_other,
    )
    first_out = lax.psum_scatter(
        mixer_term.astype(jnp.bfloat16), "tp", scatter_dimension=1, tiled=True
    )
    expert_summed = lax.psum_scatter(
        flat_term.astype(jnp.bfloat16), "tp", scatter_dimension=1, tiled=True
    )
    half_out = expert_summed.reshape(expert_count, capacity, quarter_width)
    returned = lax.all_to_all(half_out, ("z", "y"), split_axis=0, concat_axis=0, tiled=True)
    route_out = returned.reshape(-1, quarter_width).astype(jnp.float32)
    picked = route_out[positions].reshape(row_count, 2, quarter_width)
    shares = jax.nn.sigmoid(route_logits - route_logits[:, ::-1])
    second_out = jnp.sum(picked * shares[:, :, None], axis=1).astype(jnp.bfloat16)
    return (first_out, second_out)


def solution(mesh):
    split_mesh = Mesh(mesh.devices.reshape(8, 4, 2, 4), ("z", "y", "core", "tp"))
    ep = ("z", "y", "core")
    placed = (
        P(ep, None),
        P(),
        P(None, "tp"),
        P("tp", None, None),
        P("tp"),
        P("tp", None),
        P(ep, None),
        P(),
        P(ep, None),
        P(ep, None),
        P(ep, None, "tp"),
        P(ep, None, "tp"),
        P(ep, "tp", None),
    )
    return jax.shard_map(
        local,
        mesh=split_mesh,
        in_specs=placed,
        out_specs=(P(ep, "tp"), P(ep, "tp")),
        check_vma=False,
    )
```

profile of v0, /device:TPU:8, one launch (start us, length us, event | category | flops | bytes accessed | tf_op | source)
XLA Modules:
  0.0 189.3 jit_solution(17867324479856150440)
XLA Ops:
  7.2 0.0 copy-start
  7.2 0.0 copy-start.1
  7.2 0.0 all-gather.2.cloned.1.call-start
  7.2 0.0 copy-start.3
  7.2 0.0 copy-start.6
  7.3 3.0 %convert_element_type.81 = f32[256,2048]{1,0:T(8,128)} convert(bf16[256,2048]{1,0:T(8,128)(2,1)} %param.19) | non-fusion elementwise | flops 524288 | bytes 3145728 | tf_op jit(solution)/shard_map/convert_element_type | solution.py:16
  10.2 0.0 copy-done.1
  10.2 0.3 multiply_reduce_fusion
  10.5 0.0 copy-done.3
  10.5 0.1 copy.17
  10.7 0.1 eq.29
  10.8 0.1 eq.25
  11.0 0.0 copy-done.6
  11.0 0.1 dynamic-slice
  11.1 1.2 fusion.16
  12.2 0.3 broadcast_in_dim.37
  12.5 0.2 reshape.116
  12.7 1.2 reduce-window.6
  13.9 0.2 slice_reduce_fusion
  14.2 0.1 copy.16
  14.3 0.1 mul.110
  14.5 0.1 fusion.75
  14.6 2.6 %scatter_custom_fusion = bf16[576,512]{1,0:T(8,128)(2,1)S(1)} fusion(s32[512]{0:T(512)S(1)} %bitcast.40, bf16[512,512]{1,0:T(8,128)(2,1)S(1)} %reshape.116, bf16[]{:T(256)} %constant.77.clone.1), kind=kCustom, calls=%fused_computation.60 | custom fusion | bytes 589826 | tf_op jit(solution)/shard_map/scatter | solution.py:97
  17.1 0.2 reshape.99
  17.3 33.9 %all_to_all.10 = bf16[32,18,512]{2,1,0:T(8,128)(2,1)S(1)} all-to-all(bf16[32,18,512]{2,1,0:T(8,128)(2,1)S(1)} %reshape.99), channel_id=1, replica_groups=mesh['z'=8,'y'=4,'core'=2,'tp'=4] {'z','y'}, dimensions={0} | all-to-all | bytes 1179648 | tf_op jit(solution)/shard_map/all_to_all | solution.py:100
  51.3 1.0 reshape.100
  52.2 0.0 all-gather.2.cloned.1.call-update
  52.3 0.0 reduce-scatter.5.cloned.1.call-start
  52.3 0.1 collective-permute-start.1
  52.4 0.5 collective-permute-start.2
  52.9 0.1 collective-permute-start.3
  53.0 31.6 %all-gather.2.cloned.1.call-done = bf16[576,2048]{1,0:T(8,128)(2,1)} async-done(((bf16[576,512]{1,0:T(8,128)(2,1)}), bf16[576,2048]{1,0:T(8,128)(2,1)}) %all-gather.2.cloned.1.call-update) | async-done | bytes 2359312 | tf_op jit(solution)/shard_map/all_gather | solution.py:102
  84.6 4.9 %fusion.80 = f32[576,512]{1,0:T(8,128)} fusion(bf16[576,2048]{1,0:T(8,128)(2,1)} %all-gather.2.cloned.1.call-done, bf16[1,2048,512]{2,1,0:T(8,128)(2,1)} %param.23), kind=kOutput, calls=%fused_computation.98 | convolution fusion | flops 1207959552 | bytes 5636096 | tf_op jit(solution)/shard_map/dot_general | solution.py:104
  89.5 0.0 collective-permute-done.1
  89.5 0.0 copy-done.7
  89.5 4.0 %fusion.88 = f32[576,512]{1,0:T(8,128)} fusion(bf16[576,2048]{1,0:T(8,128)(2,1)S(1)} %copy-done.7, bf16[2048,512]{1,0:T(8,128)(2,1)} %collective-permute-done.1), kind=kOutput, calls=%fused_computation.104 | convolution fusion | flops 1207959552 | bytes 5636096 | tf_op jit(solution)/shard_map/dot_general | solution.py:108
  93.5 7.4 %fusion.12 = f32[576,2048]{1,0:T(8,128)} fusion(bf16[576,2048]{1,0:T(8,128)(2,1)S(1)} %copy-done.7, f32[576,512]{1,0:T(8,128)} %fusion.80, bf16[1,512,2048]{2,1,0:T(8,128)(2,1)} %param.25, bf16[1,2048,512]{2,1,0:T(8,128)(2,1)} %param.24), kind=kOutput, calls=%fused_computation.20 | convolution fusion | flops 2417688576 | bytes 12451840 | tf_op jit(solution)/shard_map/dot_general | solution.py:45
  100.9 0.0 collective-permute-done.2
  100.9 0.0 collective-permute-done.3
  100.9 8.1 %add_convert_fusion = bf16[576,2048]{1,0:T(8,128)(2,1)} fusion(f32[576,2048]{1,0:T(8,128)} %fusion.12, bf16[512,2048]{1,0:T(8,128)(2,1)} %collective-permute-done.3, f32[576,512]{1,0:T(8,128)} %fusion.88, bf16[576,2048]{1,0:T(8,128)(2,1)S(1)} %copy-done.7, bf16[2048,512]{1,0:T(8,128)(2,1)} %collective-permute-done.2), kind=kOutput, calls=%fused_computation.4 | convolution fusion | flops 2420047872 | bytes 14811136 | tf_op jit(solution)/shard_map/dot_general | solution.py:45
  109.0 0.0 reduce-scatter.5.cloned.1.call-update
  109.1 0.0 reduce-scatter.3.cloned.1.call-start
  109.1 0.6 copy-done.5
  109.7 0.9 copy-done.2
  110.6 0.5 fusion
  111.1 0.0 copy-done.8
  111.1 0.0 copy-start.10
  111.2 0.0 copy-start.9
  111.2 0.8 fusion.8
  112.0 1.9 %collective-permute-start = (bf16[15,256]{1,0:T(8,128)(2,1)S(1)}, bf16[15,256]{1,0:T(8,128)(2,1)S(1)}, u32[]{:S(2)}, u32[]{:S(2)}) collective-permute-start(bf16[15,256]{1,0:T(8,128)(2,1)S(1)} %slice.78), channel_id=1, source_target_pairs={{0,4},{4,8},{8,12},{12,16},{16,20},{20,24},{24,28},{28,32},{32,36}... | collective-permute-start | bytes 23048 | tf_op jit(solution)/shard_map/ppermute | solution.py:12
  114.0 3.0 %collective-permute-done = bf16[15,256]{1,0:T(8,128)(2,1)S(1)} collective-permute-done((bf16[15,256]{1,0:T(8,128)(2,1)S(1)}, bf16[15,256]{1,0:T(8,128)(2,1)S(1)}, u32[]{:S(2)}, u32[]{:S(2)}) %collective-permute-start) | collective-permute-done | bytes 7712 | tf_op jit(solution)/shard_map/ppermute | solution.py:12
  116.9 0.1 maximum_convert_fusion
  117.0 3.5 %convolution_convert_fusion = bf16[512,2048]{1,0:T(8,128)(2,1)} fusion(bf16[256,2048]{1,0:T(8,128)(2,1)S(1)} %copy-done, f32[256]{0:T(256)S(1)} %convert_element_type.77, bf16[512,256]{1,0:T(8,128)(2,1)S(1)} %fusion.8, f32[527,256]{1,0:T(8,128)S(1)} %maximum_convert_fusion, f32[512]{0:T(512)S(1)} %minimum_convert_fusion, pred[]{:T(512)S(6)} %gt.63, ...), kind=kOutput, calls=%fused_computation.8 | convolution fusion | flops 609878016 | bytes 11930640 | tf_op jit(solution)/shard_map/dot_general | solution.py:85
  120.5 0.0 reduce-scatter.3.cloned.1.call-update
  120.5 23.2 %reduce-scatter.5.cloned.1.call-done = bf16[576,512]{1,0:T(8,128)(2,1)} async-done(((bf16[576,2048]{1,0:T(8,128)(2,1)}), bf16[576,512]{1,0:T(8,128)(2,1)}) %reduce-scatter.5.cloned.1.call-update) | async-done | bytes 589840 | tf_op jit(solution)/shard_map/reduce_scatter | solution.py:115
  143.7 2.1 %reshape.101 = bf16[32,18,512]{2,1,0:T(8,128)(2,1)} reshape(bf16[576,512]{1,0:T(8,128)(2,1)} %reduce-scatter.5.cloned.1.call-done) | data formatting | bytes 1179648 | tf_op jit(solution)/shard_map/reshape | solution.py:118
  145.8 10.2 %all-to-all-start.1 = ((bf16[32,18,512]{2,1,0:T(8,128)(2,1)}), bf16[32,18,512]{2,1,0:T(8,128)(2,1)S(1)}, u32[]{:S(2)}, u32[]{:S(2)}) async-start(bf16[32,18,512]{2,1,0:T(8,128)(2,1)} %reshape.101), calls=%async_computation.3 | async-start | bytes 1572864 | tf_op jit(solution)/shard_map/all_to_all | solution.py:119
  156.0 0.1 rev.3
  156.1 0.1 copy.20
  156.3 22.1 %all-to-all-done.1 = bf16[32,18,512]{2,1,0:T(8,128)(2,1)S(1)} async-done(((bf16[32,18,512]{2,1,0:T(8,128)(2,1)}), bf16[32,18,512]{2,1,0:T(8,128)(2,1)S(1)}, u32[]{:S(2)}, u32[]{:S(2)}) %all-to-all-start.1) | async-done | bytes 589856 | tf_op jit(solution)/shard_map/all_to_all | solution.py:119
  178.3 0.2 reshape.103
  178.5 1.6 gather_fusion
  180.1 0.6 reshape.102
  180.8 2.1 %multiply_reduce_fusion.1 = bf16[256,512]{1,0:T(8,128)(2,1)} fusion(f32[256,2,512]{2,1,0:T(2,128)S(1)} %reshape.102, f32[256,2]{1,0:T(8,128)S(1)} %copy.20), kind=kLoop, calls=%fused_computation.19 | loop fusion | flops 393216 | bytes 1312768 | tf_op jit(solution)/shard_map/reduce_sum | solution.py:123
  (23 shorter events, 0.1 us)
Async XLA Ops:
  7.2 109.8 %copy-start = (bf16[256,2048]{1,0:T(8,128)(2,1)S(1)}, bf16[256,2048]{1,0:T(8,128)(2,1)}, u32[]{:S(2)}) copy-start(bf16[256,2048]{1,0:T(8,128)(2,1)} %param.18) | copy-start | bytes 3145732
  7.2 3.0 %copy-start.1 = (bf16[256,2048]{1,0:T(8,128)(2,1)S(1)}, bf16[256,2048]{1,0:T(8,128)(2,1)}, u32[]{:S(2)}) copy-start(bf16[256,2048]{1,0:T(8,128)(2,1)} %param.19) | copy-start | bytes 3145732
  7.2 77.5 %all-gather.2.cloned.1.call-start = ((), (), s32[]{:S(2)}) async-start(), calls=%async_computation.5 | async-start | bytes 2949120 | tf_op jit(solution)/shard_map/all_gather | solution.py:102
  7.2 3.3 %copy-start.3 = (s32[256,2]{0,1:T(2,128)S(1)}, s32[256,2]{0,1:T(2,128)}, u32[]{:S(2)}) copy-start(s32[256,2]{0,1:T(2,128)} %param.21) | copy-start | bytes 6148
  7.2 3.7 %copy-start.6 = (bf16[2048]{0:T(1024)(128)(2,1)S(1)}, bf16[2048]{0:T(1024)(128)(2,1)}, u32[]{:S(2)}) copy-start(bf16[2048]{0:T(1024)(128)(2,1)} %param.20) | copy-start | bytes 12292
  52.3 91.4 %reduce-scatter.5.cloned.1.call-start = ((), (), s32[]{:S(2)}) async-start(), calls=%async_computation.6 | async-start | bytes 2949120 | tf_op jit(solution)/shard_map/reduce_scatter | solution.py:115
  52.3 37.2 %collective-permute-start.1 = (bf16[2048,512]{1,0:T(8,128)(2,1)}, bf16[2048,512]{1,0:T(8,128)(2,1)}, u32[]{:S(2)}, u32[]{:S(2)}) collective-permute-start(bf16[2048,512]{1,0:T(8,128)(2,1)} %bitcast.43), channel_id=1, source_target_pairs={{0,4},{4,0},{1,5},{5,1},{2,6},{6,2},{3,7},{7,3},{8,12},{12,8},{9,1... | collective-permute-start | bytes 6291464 | tf_op jit(solution)/shard_map/ppermute | solution.py:68
  52.4 48.5 %collective-permute-start.2 = (bf16[2048,512]{1,0:T(8,128)(2,1)}, bf16[2048,512]{1,0:T(8,128)(2,1)}, u32[]{:S(2)}, u32[]{:S(2)}) collective-permute-start(bf16[2048,512]{1,0:T(8,128)(2,1)} %bitcast.44), channel_id=1, source_target_pairs={{0,4},{4,0},{1,5},{5,1},{2,6},{6,2},{3,7},{7,3},{8,12},{12,8},{9,1... | collective-permute-start | bytes 6291464 | tf_op jit(solution)/shard_map/ppermute | solution.py:69
  52.9 48.0 %collective-permute-start.3 = (bf16[512,2048]{1,0:T(8,128)(2,1)}, bf16[512,2048]{1,0:T(8,128)(2,1)}, u32[]{:S(2)}, u32[]{:S(2)}) collective-permute-start(bf16[512,2048]{1,0:T(8,128)(2,1)} %bitcast.45), channel_id=1, source_target_pairs={{0,4},{4,0},{1,5},{5,1},{2,6},{6,2},{3,7},{7,3},{8,12},{12,8},{9,1... | collective-permute-start | bytes 6291464 | tf_op jit(solution)/shard_map/ppermute | solution.py:70
  84.6 4.9 %copy-start.7 = (bf16[576,2048]{1,0:T(8,128)(2,1)S(1)}, bf16[576,2048]{1,0:T(8,128)(2,1)}, u32[]{:S(2)}) copy-start(bf16[576,2048]{1,0:T(8,128)(2,1)} %all-gather.2.cloned.1.call-done) | copy-start | bytes 7077892
  109.0 0.7 copy-start.5
  109.0 1.6 copy-start.2
  109.1 73.8 %reduce-scatter.3.cloned.1.call-start = ((), (), s32[]{:S(2)}) async-start(), calls=%async_computation.4 | async-start | bytes 2621440 | tf_op jit(solution)/shard_map/reduce_scatter | solution.py:112
  109.7 1.4 copy-start.8
  111.1 2.8 %copy-start.10 = (bf16[256]{0:T(256)(128)(2,1)S(1)}, bf16[256]{0:T(256)(128)(2,1)}, u32[]{:S(2)}) copy-start(bf16[256]{0:T(256)(128)(2,1)} %param.17) | copy-start | bytes 1540
  111.2 5.9 %copy-start.9 = (bf16[1,256,256]{2,1,0:T(8,128)(2,1)S(1)}, bf16[1,256,256]{2,1,0:T(8,128)(2,1)}, u32[]{:S(2)}) copy-start(bf16[1,256,256]{2,1,0:T(8,128)(2,1)} %param.16) | copy-start | bytes 393220
  112.0 5.0 %collective-permute-start = (bf16[15,256]{1,0:T(8,128)(2,1)S(1)}, bf16[15,256]{1,0:T(8,128)(2,1)S(1)}, u32[]{:S(2)}, u32[]{:S(2)}) collective-permute-start(bf16[15,256]{1,0:T(8,128)(2,1)S(1)} %slice.78), channel_id=1, source_target_pairs={{0,4},{4,8},{8,12},{12,16},{16,20},{20,24},{24,28},{28,32},{32,36}... | collective-permute-start | bytes 23048 | tf_op jit(solution)/shard_map/ppermute | solution.py:12
  120.5 35.5 %copy-start.4 = (f32[256,2]{0,1:T(2,128)S(1)}, f32[256,2]{0,1:T(2,128)}, u32[]{:S(2)}) copy-start(f32[256,2]{0,1:T(2,128)} %param.22) | copy-start | bytes 6148
  145.8 32.5 %all-to-all-start.1 = ((bf16[32,18,512]{2,1,0:T(8,128)(2,1)}), bf16[32,18,512]{2,1,0:T(8,128)(2,1)S(1)}, u32[]{:S(2)}, u32[]{:S(2)}) async-start(bf16[32,18,512]{2,1,0:T(8,128)(2,1)} %reshape.101), calls=%async_computation.3 | async-start | bytes 1572864 | tf_op jit(solution)/shard_map/all_to_all | solution.py:119
Sparse Core Ops, SparseCore 0:
  52.4 32.2 all-gather.1
  109.2 34.4 reduce-scatter.4
  146.8 31.9 reduce-scatter.2
where the time goes:
time: 190 us; the launch traced here: 189 us
  waiting for transfers between devices  79.9 us (42%)
  blocking collectives  33.9 us (18%)
  matrix products  28.7 us (15%)
  between operations  14.1 us (7%)
  starting transfers between devices  12.9 us (7%)
  local copies, waits for them, and re-layouts  11.5 us (6%)
  other arithmetic  8.35 us (4%)
    all_to_all x1, blocking collectives, local(): lax.all_to_all(buffer, ('z', 'y'), split_axis=0, concat_axis=0, tiled=True)  33.9 us
    all_gather x1, waiting for transfers between devices, local(): portion = lax.all_gather(flattened, 'tp', axis=1, tiled=True)  31.6 us
    reduce_scatter x1, waiting for transfers between devices, local(): lax.psum_scatter(flat_term.astype(jnp.bfloat16), 'tp', scatter_dimension=...  23.2 us
    all_to_all x1, waiting for transfers between devices, local(): lax.all_to_all(half_out, ('z', 'y'), split_axis=0, concat_axis=0, tiled=T...  22.1 us
    dot_general x2, matrix products, expert_output(): return jnp.dot(hidden, down_rows, preferred_element_type=jnp.float32)  15.5 us
    all_to_all x1, starting transfers between devices, local(): lax.all_to_all(half_out, ('z', 'y'), split_axis=0, concat_axis=0, tiled=T...  10.2 us
    dot_general x1, matrix products, local(): jnp.dot(portion, expert_gate[0], preferred_element_type=jnp.float32)  4.89 us
    dot_general x1, matrix products, local(): jnp.dot(portion, gate_other, preferred_element_type=jnp.float32)  3.97 us
  transfers between devices with their start and end apart: 8, of which 4 were waited for; matrix products, arithmetic and copies ran while one was open for 15% of the time, Pallas kernels for 0%

commit v1 on v0

--- a/solution.py
+++ b/solution.py
@@ -2,6 +2,7 @@
 import jax.numpy as jnp
 from jax import lax
 from jax.sharding import Mesh, PartitionSpec as P
+from jax.lax import all_to_all, axis_size
 
 epsilon = 1e-06
 
@@ -99,7 +100,14 @@
     )
     arrived = lax.all_to_all(buffer, ("z", "y"), split_axis=0, concat_axis=0, tiled=True)
     flattened = arrived.reshape(-1, quarter_width)
-    portion = lax.all_gather(flattened, "tp", axis=1, tiled=True)
+
+    def edge_turn(raw, device_axis):
+        odd = all_to_all(
+            jnp.concatenate([raw] * axis_size(device_axis), axis=1), device_axis, 1, 1, tiled=True
+        )
+        return odd
+
+    portion = edge_turn(flattened, "tp")
     flat_term = expert_output(
         jnp.dot(portion, expert_gate[0], preferred_element_type=jnp.float32),
         jnp.dot(portion, expert_up[0], preferred_element_type=jnp.float32),

time: 190 us -> 184 us (0.968)
  waiting for transfers between devices: 79.9 us -> 70.4 us
  starting transfers between devices: 12.9 us -> 17 us
  local copies, waits for them, and re-layouts: 11.5 us -> 14.7 us
  other arithmetic: 8.35 us -> 5.95 us
    all_gather x1 -> x0, waiting for transfers between devices: 31.6 us -> none  [local(): portion = lax.all_gather(flattened, 'tp', axis=1, tiled=True)]
    all_to_all x0 -> x1, waiting for transfers between devices: none -> 26.9 us  [edge_turn(): all_to_all(jnp.concatenate([raw] * axis_size(device_axis), axis=1), devic...]
    reduce_scatter x1, waiting for transfers between devices: 23.2 us -> 18.4 us  [local(): lax.psum_scatter(flat_term.astype(jnp.bfloat16), 'tp', scatter_dimension=...]
    all_to_all x0 -> x1, starting transfers between devices: none -> 4.29 us  [edge_turn(): all_to_all(jnp.concatenate([raw] * axis_size(device_axis), axis=1), devic...]
    dot_general x1, matrix products: 4.89 us -> 2.47 us  [local(): jnp.dot(portion, expert_gate[0], preferred_element_type=jnp.float32)]
    unnamed x23 -> x27, local copies, waits for them, and re-layouts: 1.71 us -> 3.81 us
where the time goes in v1:
time: 184 us
  waiting for transfers between devices  70.4 us (38%)
  blocking collectives  33.9 us (18%)
  matrix products  27.1 us (15%)
  starting transfers between devices  17 us (9%)
  local copies, waits for them, and re-layouts  14.7 us (8%)
  between operations  14.4 us (8%)
  other arithmetic  5.95 us (3%)
    all_to_all x1, blocking collectives, local(): lax.all_to_all(buffer, ('z', 'y'), split_axis=0, concat_axis=0, tiled=True)  33.9 us
    all_to_all x1, waiting for transfers between devices, edge_turn(): all_to_all(jnp.concatenate([raw] * axis_size(device_axis), axis=1), devic...  26.9 us
    all_to_all x1, waiting for transfers between devices, local(): lax.all_to_all(half_out, ('z', 'y'), split_axis=0, concat_axis=0, tiled=T...  22.1 us
    reduce_scatter x1, waiting for transfers between devices, local(): lax.psum_scatter(flat_term.astype(jnp.bfloat16), 'tp', scatter_dimension=...  18.4 us
    dot_general x2, matrix products, expert_output(): return jnp.dot(hidden, down_rows, preferred_element_type=jnp.float32)  16.4 us
    all_to_all x1, starting transfers between devices, local(): lax.all_to_all(half_out, ('z', 'y'), split_axis=0, concat_axis=0, tiled=T...  10.2 us
    all_to_all x1, starting transfers between devices, edge_turn(): all_to_all(jnp.concatenate([raw] * axis_size(device_axis), axis=1), devic...  4.29 us
    dot_general x1, matrix products, local(): jnp.dot(portion, gate_other, preferred_element_type=jnp.float32)  3.99 us
  transfers between devices with their start and end apart: 8, of which 4 were waited for; matrix products, arithmetic and copies ran while one was open for 15% of the time, Pallas kernels for 0%

profile of v1, /device:TPU:8, one launch (start us, length us, event | category | flops | bytes accessed | tf_op | source)
XLA Modules:
  0.0 183.6 jit_solution(6292548652725823668)
XLA Ops:
  7.2 0.0 copy-start
  7.2 0.0 copy-start.1
  7.2 0.0 copy-start.5
  7.2 0.0 copy-start.8
  7.2 1.6 convert_element_type.81
  8.8 0.0 copy-done.1
  8.8 0.3 multiply_reduce_fusion
  9.1 0.0 copy-done.5
  9.1 0.1 copy.27
  9.3 0.1 eq.29
  9.4 0.1 eq.25
  9.6 0.1 dynamic-slice
  9.7 0.1 fusion.16
  9.8 0.3 broadcast_in_dim.37
  10.1 0.2 reshape.125
  10.3 1.2 reduce-window.6
  11.5 0.2 slice_reduce_fusion
  11.7 0.1 copy.26
  11.9 0.1 mul.110
  12.0 0.1 fusion.75
  12.1 2.6 %scatter_custom_fusion = bf16[576,512]{1,0:T(8,128)(2,1)S(1)} fusion(s32[512]{0:T(512)S(1)} %bitcast.47, bf16[512,512]{1,0:T(8,128)(2,1)S(1)} %reshape.125, bf16[]{:T(256)} %constant.77.clone.1), kind=kCustom, calls=%fused_computation.60 | custom fusion | bytes 589826 | tf_op jit(solution)/shard_map/scatter | solution.py:98
  14.7 0.2 reshape.109
  14.9 33.9 %all_to_all.19 = bf16[32,18,512]{2,1,0:T(8,128)(2,1)S(1)} all-to-all(bf16[32,18,512]{2,1,0:T(8,128)(2,1)S(1)} %reshape.109), channel_id=1, replica_groups=mesh['z'=8,'y'=4,'core'=2,'tp'=4] {'z','y'}, dimensions={0} | all-to-all | bytes 1179648 | tf_op jit(solution)/shard_map/all_to_all | solution.py:101
  48.8 0.2 concatenate.10
  49.0 1.6 concatenate.11
  50.6 4.3 %all-to-all-start.1 = ((bf16[576,4,512]{2,0,1:T(8,128)(2,1)}), bf16[576,4,512]{2,0,1:T(8,128)(2,1)S(1)}, u32[]{:S(2)}, u32[]{:S(2)}) async-start(bf16[576,4,512]{2,0,1:T(8,128)(2,1)} %concatenate.11), calls=%async_computation.2 | async-start | bytes 4718592 | tf_op jit(solution)/shard_map/all_to_all | solution.py:105
  54.9 0.0 collective-permute-start.1
  54.9 0.5 collective-permute-start.2
  55.4 0.1 collective-permute-start.3
  55.5 26.9 %all-to-all-done.1 = bf16[576,4,512]{2,0,1:T(8,128)(2,1)S(1)} async-done(((bf16[576,4,512]{2,0,1:T(8,128)(2,1)}), bf16[576,4,512]{2,0,1:T(8,128)(2,1)S(1)}, u32[]{:S(2)}, u32[]{:S(2)}) %all-to-all-start.1) | async-done | bytes 2359328 | tf_op jit(solution)/shard_map/all_to_all | solution.py:105
  82.4 0.3 copy.33
  82.7 2.1 %copy-done.9 = bf16[1,2048,512]{2,1,0:T(8,128)(2,1)S(1)} copy-done((bf16[1,2048,512]{2,1,0:T(8,128)(2,1)S(1)}, bf16[1,2048,512]{2,1,0:T(8,128)(2,1)}, u32[]{:S(2)}) %copy-start.9) | copy-done | bytes 2097176
  84.8 2.5 %fusion.80 = f32[576,512]{1,0:T(8,128)} fusion(bf16[576,2048]{1,0:T(8,128)(2,1)S(1)} %bitcast.43, bf16[1,2048,512]{2,1,0:T(8,128)(2,1)S(1)} %copy-done.9), kind=kOutput, calls=%fused_computation.98 | convolution fusion | flops 1207959552 | bytes 5636096 | tf_op jit(solution)/shard_map/dot_general | solution.py:112
  87.3 0.0 collective-permute-done.1
  87.3 4.0 %fusion.88 = f32[576,512]{1,0:T(8,128)} fusion(bf16[576,2048]{1,0:T(8,128)(2,1)S(1)} %bitcast.44, bf16[2048,512]{1,0:T(8,128)(2,1)} %collective-permute-done.1), kind=kOutput, calls=%fused_computation.104 | convolution fusion | flops 1207959552 | bytes 5636096 | tf_op jit(solution)/shard_map/dot_general | solution.py:116
  91.3 8.3 %fusion.12 = f32[576,2048]{1,0:T(8,128)} fusion(bf16[576,2048]{1,0:T(8,128)(2,1)} %bitcast.45, f32[576,512]{1,0:T(8,128)} %fusion.80, bf16[1,512,2048]{2,1,0:T(8,128)(2,1)} %param.25, bf16[1,2048,512]{2,1,0:T(8,128)(2,1)} %param.24), kind=kOutput, calls=%fused_computation.20 | convolution fusion | flops 2417688576 | bytes 12451840 | tf_op jit(solution)/shard_map/dot_general | solution.py:46
  99.5 0.0 collective-permute-done.2
  99.6 0.0 collective-permute-done.3
  99.6 8.1 %add_convert_fusion = bf16[576,2048]{1,0:T(8,128)(2,1)} fusion(f32[576,2048]{1,0:T(8,128)} %fusion.12, bf16[512,2048]{1,0:T(8,128)(2,1)} %collective-permute-done.3, f32[576,512]{1,0:T(8,128)} %fusion.88, bf16[576,2048]{1,0:T(8,128)(2,1)S(1)} %bitcast.46, bf16[2048,512]{1,0:T(8,128)(2,1)} %collective-permute-done.2), kind=kOutput, calls=%fused_computation.4 | convolution fusion | flops 2420047872 | bytes 14811136 | tf_op jit(solution)/shard_map/dot_general | solution.py:46
  107.7 0.0 reduce-scatter.5.cloned.1.call-update
  107.7 0.0 reduce-scatter.3.cloned.1.call-start
  107.7 0.6 copy-done.7
  108.4 0.9 copy-done.4
  109.3 0.5 fusion
  109.8 0.0 copy-done.10
  109.8 0.0 copy-start.12
  109.8 0.0 copy-start.11
  109.8 0.8 fusion.8
  110.6 1.9 %collective-permute-start = (bf16[15,256]{1,0:T(8,128)(2,1)S(1)}, bf16[15,256]{1,0:T(8,128)(2,1)S(1)}, u32[]{:S(2)}, u32[]{:S(2)}) collective-permute-start(bf16[15,256]{1,0:T(8,128)(2,1)S(1)} %slice.78), channel_id=1, source_target_pairs={{0,4},{4,8},{8,12},{12,16},{16,20},{20,24},{24,28},{28,32},{32,36}... | collective-permute-start | bytes 23048 | tf_op jit(solution)/shard_map/ppermute | solution.py:13
  112.6 3.0 %collective-permute-done = bf16[15,256]{1,0:T(8,128)(2,1)S(1)} collective-permute-done((bf16[15,256]{1,0:T(8,128)(2,1)S(1)}, bf16[15,256]{1,0:T(8,128)(2,1)S(1)}, u32[]{:S(2)}, u32[]{:S(2)}) %collective-permute-start) | collective-permute-done | bytes 7712 | tf_op jit(solution)/shard_map/ppermute | solution.py:13
  115.6 0.1 maximum_convert_fusion
  115.7 3.5 %convolution_convert_fusion = bf16[512,2048]{1,0:T(8,128)(2,1)} fusion(bf16[256,2048]{1,0:T(8,128)(2,1)S(1)} %copy-done, f32[256]{0:T(256)S(1)} %convert_element_type.77, bf16[512,256]{1,0:T(8,128)(2,1)S(1)} %fusion.8, f32[527,256]{1,0:T(8,128)S(1)} %maximum_convert_fusion, f32[512]{0:T(512)S(1)} %minimum_convert_fusion, pred[]{:T(512)S(6)} %gt.63, ...), kind=kOutput, calls=%fused_computation.8 | convolution fusion | flops 609878016 | bytes 11930640 | tf_op jit(solution)/shard_map/dot_general | solution.py:86
  119.2 0.0 reduce-scatter.3.cloned.1.call-update
  119.2 18.4 %reduce-scatter.5.cloned.1.call-done = bf16[576,512]{1,0:T(8,128)(2,1)} async-done(((bf16[576,2048]{1,0:T(8,128)(2,1)}), bf16[576,512]{1,0:T(8,128)(2,1)}) %reduce-scatter.5.cloned.1.call-update) | async-done | bytes 589840 | tf_op jit(solution)/shard_map/reduce_scatter | solution.py:123
  137.6 2.1 %reshape.110 = bf16[32,18,512]{2,1,0:T(8,128)(2,1)} reshape(bf16[576,512]{1,0:T(8,128)(2,1)} %reduce-scatter.5.cloned.1.call-done) | data formatting | bytes 1179648 | tf_op jit(solution)/shard_map/reshape | solution.py:126
  139.7 10.2 %all-to-all-start.2 = ((bf16[32,18,512]{2,1,0:T(8,128)(2,1)}), bf16[32,18,512]{2,1,0:T(8,128)(2,1)S(1)}, u32[]{:S(2)}, u32[]{:S(2)}) async-start(bf16[32,18,512]{2,1,0:T(8,128)(2,1)} %reshape.110), calls=%async_computation.4 | async-start | bytes 1572864 | tf_op jit(solution)/shard_map/all_to_all | solution.py:127
  149.8 0.0 copy-done.6
  149.9 0.1 rev.3
  150.0 0.1 copy.31
  150.1 22.1 %all-to-all-done.2 = bf16[32,18,512]{2,1,0:T(8,128)(2,1)S(1)} async-done(((bf16[32,18,512]{2,1,0:T(8,128)(2,1)}), bf16[32,18,512]{2,1,0:T(8,128)(2,1)S(1)}, u32[]{:S(2)}, u32[]{:S(2)}) %all-to-all-start.2) | async-done | bytes 589856 | tf_op jit(solution)/shard_map/all_to_all | solution.py:127
  172.2 0.2 reshape.112
  172.4 1.6 gather_fusion
  174.0 0.6 reshape.111
  174.7 2.1 %multiply_reduce_fusion.1 = bf16[256,512]{1,0:T(8,128)(2,1)} fusion(f32[256,2,512]{2,1,0:T(2,128)S(1)} %reshape.111, f32[256,2]{1,0:T(8,128)S(1)} %copy.31), kind=kLoop, calls=%fused_computation.19 | loop fusion | flops 393216 | bytes 1312768 | tf_op jit(solution)/shard_map/reduce_sum | solution.py:131
  (28 shorter events, 0.1 us)
Async XLA Ops:
  7.2 108.5 %copy-start = (bf16[256,2048]{1,0:T(8,128)(2,1)S(1)}, bf16[256,2048]{1,0:T(8,128)(2,1)}, u32[]{:S(2)}) copy-start(bf16[256,2048]{1,0:T(8,128)(2,1)} %param.18) | copy-start | bytes 3145732
  7.2 1.6 copy-start.1
  7.2 1.9 %copy-start.5 = (s32[256,2]{0,1:T(2,128)S(1)}, s32[256,2]{0,1:T(2,128)}, u32[]{:S(2)}) copy-start(s32[256,2]{0,1:T(2,128)} %param.21) | copy-start | bytes 6148
  7.2 2.4 %copy-start.8 = (bf16[2048]{0:T(1024)(128)(2,1)S(1)}, bf16[2048]{0:T(1024)(128)(2,1)}, u32[]{:S(2)}) copy-start(bf16[2048]{0:T(1024)(128)(2,1)} %param.20) | copy-start | bytes 12292
  50.6 31.8 %all-to-all-start.1 = ((bf16[576,4,512]{2,0,1:T(8,128)(2,1)}), bf16[576,4,512]{2,0,1:T(8,128)(2,1)S(1)}, u32[]{:S(2)}, u32[]{:S(2)}) async-start(bf16[576,4,512]{2,0,1:T(8,128)(2,1)} %concatenate.11), calls=%async_computation.2 | async-start | bytes 4718592 | tf_op jit(solution)/shard_map/all_to_all | solution.py:105
  54.9 82.7 %reduce-scatter.5.cloned.1.call-start = ((), (), s32[]{:S(2)}) async-start(), calls=%async_computation.6 | async-start | bytes 2949120 | tf_op jit(solution)/shard_map/reduce_scatter | solution.py:123
  54.9 32.4 %collective-permute-start.1 = (bf16[2048,512]{1,0:T(8,128)(2,1)}, bf16[2048,512]{1,0:T(8,128)(2,1)}, u32[]{:S(2)}, u32[]{:S(2)}) collective-permute-start(bf16[2048,512]{1,0:T(8,128)(2,1)} %bitcast.50), channel_id=1, source_target_pairs={{0,4},{4,0},{1,5},{5,1},{2,6},{6,2},{3,7},{7,3},{8,12},{12,8},{9,1... | collective-permute-start | bytes 6291464 | tf_op jit(solution)/shard_map/ppermute | solution.py:69
  54.9 44.6 %collective-permute-start.2 = (bf16[2048,512]{1,0:T(8,128)(2,1)}, bf16[2048,512]{1,0:T(8,128)(2,1)}, u32[]{:S(2)}, u32[]{:S(2)}) collective-permute-start(bf16[2048,512]{1,0:T(8,128)(2,1)} %bitcast.51), channel_id=1, source_target_pairs={{0,4},{4,0},{1,5},{5,1},{2,6},{6,2},{3,7},{7,3},{8,12},{12,8},{9,1... | collective-permute-start | bytes 6291464 | tf_op jit(solution)/shard_map/ppermute | solution.py:70
  55.4 44.1 %collective-permute-start.3 = (bf16[512,2048]{1,0:T(8,128)(2,1)}, bf16[512,2048]{1,0:T(8,128)(2,1)}, u32[]{:S(2)}, u32[]{:S(2)}) collective-permute-start(bf16[512,2048]{1,0:T(8,128)(2,1)} %bitcast.52), channel_id=1, source_target_pairs={{0,4},{4,0},{1,5},{5,1},{2,6},{6,2},{3,7},{7,3},{8,12},{12,8},{9,1... | collective-permute-start | bytes 6291464 | tf_op jit(solution)/shard_map/ppermute | solution.py:71
  82.4 2.4 %copy-start.9 = (bf16[1,2048,512]{2,1,0:T(8,128)(2,1)S(1)}, bf16[1,2048,512]{2,1,0:T(8,128)(2,1)}, u32[]{:S(2)}) copy-start(bf16[1,2048,512]{2,1,0:T(8,128)(2,1)} %param.23) | copy-start | bytes 6291460
  82.7 4.6 %copy-start.2 = (bf16[4,72,8,512]{3,2,0,1:T(8,128)(2,1)}, bf16[4,72,8,512]{3,2,0,1:T(8,128)(2,1)S(1)}, u32[]{:S(2)}) copy-start(bf16[4,72,8,512]{3,2,0,1:T(8,128)(2,1)S(1)} %copy.33) | copy-start | bytes 7077892
  91.3 8.3 %copy-start.3 = (bf16[4,72,8,512]{3,2,0,1:T(8,128)(2,1)S(1)}, bf16[4,72,8,512]{3,2,0,1:T(8,128)(2,1)}, u32[]{:S(2)}) copy-start(bf16[4,72,8,512]{3,2,0,1:T(8,128)(2,1)} %copy-done.2) | copy-start | bytes 7077892
  107.7 0.7 copy-start.7
  107.7 1.6 copy-start.4
  107.7 69.0 %reduce-scatter.3.cloned.1.call-start = ((), (), s32[]{:S(2)}) async-start(), calls=%async_computation.5 | async-start | bytes 2621440 | tf_op jit(solution)/shard_map/reduce_scatter | solution.py:120
  108.4 1.4 copy-start.10
  109.8 2.8 %copy-start.12 = (bf16[256]{0:T(256)(128)(2,1)S(1)}, bf16[256]{0:T(256)(128)(2,1)}, u32[]{:S(2)}) copy-start(bf16[256]{0:T(256)(128)(2,1)} %param.17) | copy-start | bytes 1540
  109.8 5.9 %copy-start.11 = (bf16[1,256,256]{2,1,0:T(8,128)(2,1)S(1)}, bf16[1,256,256]{2,1,0:T(8,128)(2,1)}, u32[]{:S(2)}) copy-start(bf16[1,256,256]{2,1,0:T(8,128)(2,1)} %param.16) | copy-start | bytes 393220
  110.6 5.0 %collective-permute-start = (bf16[15,256]{1,0:T(8,128)(2,1)S(1)}, bf16[15,256]{1,0:T(8,128)(2,1)S(1)}, u32[]{:S(2)}, u32[]{:S(2)}) collective-permute-start(bf16[15,256]{1,0:T(8,128)(2,1)S(1)} %slice.78), channel_id=1, source_target_pairs={{0,4},{4,8},{8,12},{12,16},{16,20},{20,24},{24,28},{28,32},{32,36}... | collective-permute-start | bytes 23048 | tf_op jit(solution)/shard_map/ppermute | solution.py:13
  119.2 30.7 %copy-start.6 = (f32[256,2]{0,1:T(2,128)S(1)}, f32[256,2]{0,1:T(2,128)}, u32[]{:S(2)}) copy-start(f32[256,2]{0,1:T(2,128)} %param.22) | copy-start | bytes 6148
  139.7 32.5 %all-to-all-start.2 = ((bf16[32,18,512]{2,1,0:T(8,128)(2,1)}), bf16[32,18,512]{2,1,0:T(8,128)(2,1)S(1)}, u32[]{:S(2)}, u32[]{:S(2)}) async-start(bf16[32,18,512]{2,1,0:T(8,128)(2,1)} %reshape.110), calls=%async_computation.4 | async-start | bytes 1572864 | tf_op jit(solution)/shard_map/all_to_all | solution.py:127
Sparse Core Ops, SparseCore 0:
  107.8 29.7 reduce-scatter.4
  140.7 32.0 reduce-scatter.2
